TPU v7x, 32 devices: a whole 2x2x4 slice. The times are simulated.
32 devices in a mesh: ep: 16 (over z, y, x), tp: 2 (over core).
Axes of the slice: x: 2, y: 2, z: 4, core: 2. Of those that a mesh axis runs over, the one named last changes fastest.
Arguments:
- tokens: bfloat16 [1024, 2048], P('ep', 'tp'), may hold values from -6 to 6
- sequence_state_real: float32 [1024, 128, 64], P('ep', 'tp'), may hold values from -4 to 4
- sequence_state_imaginary: float32 [1024, 128, 64], P('ep', 'tp'), may hold values from -4 to 4
- mixer_norm_gain: float32 [2048], replicated, may hold values from 0.1 to 1.9
- expert_norm_gain: float32 [2048], replicated, may hold values from 0.1 to 1.9
- rate: float32 [128, 64], P('tp'), may hold values from 0.1 to 4
- freq: float32 [128, 64], P('tp'), may hold values from -3 to 3
- log_group_step: float32 [128], P('tp'), may hold values from -3 to 0
- input_map_real: float32 [128, 64, 16], P('tp'), may hold values from -1 to 1
- input_map_imaginary: float32 [128, 64, 16], P('tp'), may hold values from -1 to 1
- output_map_real: float32 [128, 16, 64], P('tp'), may hold values from -0.75 to 0.75
- output_map_imaginary: float32 [128, 16, 64], P('tp'), may hold values from -0.75 to 0.75
- skip: float32 [2048], P('tp'), may hold values from -4 to 4
- mixer_value_weight: bfloat16 [2048, 2048], P('tp'), may hold values from -0.125 to 0.125
- mixer_gate_weight: bfloat16 [2048, 2048], P('tp'), may hold values from -0.125 to 0.125
- group_router_weight: bfloat16 [2048, 4], replicated, may hold values from -0.125 to 0.125
- expert_router_weight: bfloat16 [2048, 16], replicated, may hold values from -0.125 to 0.125
- dense_blend_weight: float32 [2048], replicated, may hold values from -0.125 to 0.125
- routes: int32 [1024, 2], P('ep'), may hold values from 0 to 15, all different within a row; in each aligned block of 64 rows (0 to 63, 64 to 127, ...) at most 16 rows name the same one
- expert_gate_weight: bfloat16 [16, 2048, 1024], P('ep', None, 'tp'), may hold values from -0.125 to 0.125
- expert_up_weight: bfloat16 [16, 2048, 1024], P('ep', None, 'tp'), may hold values from -0.125 to 0.125
- expert_down_weight: bfloat16 [16, 1024, 2048], P('ep', 'tp'), may hold values from -0.1875 to 0.1875
- shared_gate_weight: bfloat16 [2048, 2048], P('tp', 'ep'), may hold values from -0.125 to 0.125
- shared_up_weight: bfloat16 [2048, 2048], P('tp', 'ep'), may hold values from -0.125 to 0.125
- shared_down_weight: bfloat16 [2048, 2048], P(None, 'tp'), may hold values from -0.125 to 0.125
Outputs:
- result: bfloat16 [1024, 2048], P('ep', 'tp')
- next_re: float32 [1024, 128, 64], P('ep', 'tp')
- next_im: float32 [1024, 128, 64], P('ep', 'tp')
Inputs may be any that keep to these rules, and one draw needn't show every extreme that they name: `routes`: each row names 2 different experts. Among the rows of one device no expert is named more than 16 times, and in every draw some expert is named exactly 16 times by some device's rows.
All inputs are finite; a program needn't handle non-finite values.
Results may differ from a plain program's by a relative error of at most 0.017.
Values may be sent and summed in bfloat16 or wider, within the bound.
A program may use at most 128 MiB of HBM per device.

v0:
```python
import jax
import jax.numpy as jnp
from jax import lax
from jax.sharding import PartitionSpec as P

NG = 4
EPS = 1e-06
PRECISION_MAX = lax.Precision.HIGHEST


def state_factors(rate, freq, log_group_step, input_map_real, input_map_imaginary):
    step_size = jnp.exp(log_group_step)[:, None]
    magnitude = jnp.exp(-rate * step_size)
    abar_re = magnitude * jnp.cos(freq * step_size)
    abar_im = magnitude * jnp.sin(freq * step_size)
    denom = rate * rate + freq * freq
    shift_re = abar_re - 1.0
    fac_re = (abar_im * freq - shift_re * rate) / denom
    fac_im = -(abar_im * rate + shift_re * freq) / denom
    bbar_re = fac_re[:, :, None] * input_map_real - fac_im[:, :, None] * input_map_imaginary
    bbar_im = fac_re[:, :, None] * input_map_imaginary + fac_im[:, :, None] * input_map_real
    return (abar_re, abar_im, bbar_re, bbar_im)


def state_step(
    normed,
    sequence_state_real,
    sequence_state_imaginary,
    factors,
    output_map_real,
    output_map_imaginary,
    skip,
):
    abar_re, abar_im, bbar_re, bbar_im = factors
    groups = abar_re.shape[0]
    inputs = normed.astype(jnp.float32)
    grouped = inputs.reshape(inputs.shape[0], groups, -1)
    drive_re = jnp.einsum("tgc,gpc->tgp", grouped, bbar_re, precision=PRECISION_MAX)
    drive_im = jnp.einsum("tgc,gpc->tgp", grouped, bbar_im, precision=PRECISION_MAX)
    fresh_real = abar_re * sequence_state_real - abar_im * sequence_state_imaginary + drive_re
    fresh_imaginary = abar_re * sequence_state_imaginary + abar_im * sequence_state_real + drive_im
    state_readout = jnp.einsum("dor,zdr->zdo", output_map_real, fresh_real, precision=PRECISION_MAX)
    state_readout = state_readout - jnp.einsum(
        "dor,zdr->zdo", output_map_imaginary, fresh_imaginary, precision=PRECISION_MAX
    )
    mixed = state_readout.reshape(inputs.shape) + skip * inputs
    return (mixed, fresh_real, fresh_imaginary)


def pair_product(left, first_map, second_map):
    first = jnp.dot(left, first_map, preferred_element_type=jnp.float32)
    second = jnp.dot(left, second_map, preferred_element_type=jnp.float32)
    return jnp.concatenate([first, second], axis=1)


def shards(
    tokens,
    sequence_state_real,
    sequence_state_imaginary,
    mixer_norm_gain,
    expert_norm_gain,
    rate,
    freq,
    log_group_step,
    input_map_real,
    input_map_imaginary,
    output_map_real,
    output_map_imaginary,
    skip,
    mixer_value_weight,
    mixer_gate_weight,
    group_router_weight,
    expert_router_weight,
    dense_blend_weight,
    routes,
    expert_gate_weight,
    expert_up_weight,
    expert_down_weight,
    shared_gate_weight,
    shared_up_weight,
    shared_down_weight,
):
    seq_rows, half_width = tokens.shape
    width = 2 * half_width
    column_start = lax.axis_index("tp") * half_width

    def own_rows(values):
        return lax.dynamic_slice_in_dim(values, column_start, half_width, 0)

    float_tokens = tokens.astype(jnp.float32)
    square_sum = lax.psum(jnp.sum(float_tokens * float_tokens, axis=1), "tp")
    first_scale = lax.rsqrt(square_sum / width + EPS)[:, None]
    normed = (float_tokens * first_scale * own_rows(mixer_norm_gain)).astype(jnp.bfloat16)
    factors = state_factors(rate, freq, log_group_step, input_map_real, input_map_imaginary)
    mixed, next_re, next_im = state_step(
        normed,
        sequence_state_real,
        sequence_state_imaginary,
        factors,
        output_map_real,
        output_map_imaginary,
        skip,
    )
    activated = jax.nn.gelu(mixed).astype(jnp.bfloat16)
    value_part = jnp.dot(activated, mixer_value_weight, preferred_element_type=jnp.float32)
    gate_part = jnp.dot(activated, mixer_gate_weight, preferred_element_type=jnp.float32)
    stacked = jnp.stack([value_part, gate_part], axis=1)
    mix_sum = lax.psum_scatter(
        stacked.astype(jnp.bfloat16), "tp", scatter_dimension=2, tiled=True
    ).astype(jnp.float32)
    mix_half = (mix_sum[:, 0] * jax.nn.sigmoid(mix_sum[:, 1])).astype(jnp.bfloat16)
    hidden = (float_tokens + mix_half.astype(jnp.float32)).astype(jnp.bfloat16)
    hidden_f32 = hidden.astype(jnp.float32)
    scaled = hidden_f32 * own_rows(expert_norm_gain)
    router_map = jnp.concatenate(
        [own_rows(group_router_weight), own_rows(expert_router_weight)], axis=1
    ).astype(jnp.float32)
    blend_map = own_rows(dense_blend_weight)
    hidden_squares = jnp.sum(hidden_f32 * hidden_f32, axis=1)
    total_squares = lax.psum(hidden_squares, "tp")
    inverse = lax.rsqrt(total_squares / width + EPS)[:, None]
    normal_rows = scaled * inverse
    raw_part = jnp.dot(normal_rows, router_map, precision=PRECISION_MAX)
    blend_part = jnp.dot(normal_rows, blend_map, precision=PRECISION_MAX)
    logits, blend_logit = lax.psum((raw_part, blend_part), "tp")
    hnorm = (scaled * inverse).astype(jnp.bfloat16)
    experts = expert_router_weight.shape[1]
    top_count = routes.shape[1]
    per_group = experts // NG
    group_prob = jax.nn.softmax(logits[:, :NG], axis=-1)
    expert_logits = logits[:, NG:]
    expert_hits = routes[:, :, None] == jnp.arange(experts, dtype=jnp.int32)[None, None, :]
    chosen = jnp.sum(jnp.where(expert_hits, expert_logits[:, None, :], 0.0), axis=2)
    group_hits = (routes // per_group)[:, :, None] == jnp.arange(NG, dtype=jnp.int32)[None, None, :]
    group_sel = jnp.sum(jnp.where(group_hits, group_prob[:, None, :], 0.0), axis=2)
    weights = jax.nn.softmax(chosen, axis=1) * group_sel
    full_rows = lax.all_gather(hnorm, "tp", axis=1, tiled=True)
    capacity = max(2, 2 * seq_rows * top_count // experts)
    flat_routes = routes.reshape(-1)
    matches = (flat_routes[:, None] == jnp.arange(experts, dtype=jnp.int32)[None, :]).astype(
        jnp.int32
    )
    slot_rank = jnp.sum(jnp.cumsum(matches, axis=0) * matches, axis=1) - 1
    slot_target = flat_routes * capacity + slot_rank
    dispatch = slot_target[None, :] == jnp.arange(experts * capacity, dtype=jnp.int32)[:, None]
    dispatch_rows = jnp.sum(
        dispatch.reshape(experts * capacity, seq_rows, top_count).astype(jnp.float32), axis=2
    )
    outgoing = jnp.dot(
        dispatch_rows.astype(jnp.bfloat16), full_rows, preferred_element_type=jnp.float32
    )
    outgoing = outgoing.astype(jnp.bfloat16).reshape(experts, capacity, width)
    received = lax.all_to_all(outgoing, "ep", split_axis=0, concat_axis=0, tiled=True)
    sources = received.shape[0]
    items = received.shape[1]
    token_rows = received.reshape(sources * items, width)
    gate_e = jnp.dot(token_rows, expert_gate_weight[0], preferred_element_type=jnp.float32)
    expert_up_rows = jnp.dot(token_rows, expert_up_weight[0], preferred_element_type=jnp.float32)
    inner = (jax.nn.silu(gate_e) * expert_up_rows).astype(jnp.bfloat16)
    part_out = jnp.dot(inner, expert_down_weight[0], preferred_element_type=jnp.float32)
    total = lax.psum_scatter(part_out.astype(jnp.bfloat16), "tp", scatter_dimension=1, tiled=True)
    finished = total.reshape(sources, items, half_width)
    returned = lax.all_to_all(finished, "ep", split_axis=0, concat_axis=0, tiled=True)
    returned_flat = returned.reshape(experts * capacity, half_width)
    picked = returned_flat[slot_target].reshape(seq_rows, top_count, half_width).astype(jnp.float32)
    routed = jnp.sum(weights[:, :, None] * picked, axis=1)
    partial_dense = pair_product(
        lax.all_gather(hnorm, "ep", axis=0, tiled=True), shared_gate_weight, shared_up_weight
    )
    dense_sum = lax.psum(partial_dense.astype(jnp.bfloat16), "tp").astype(jnp.float32)
    dense_cols = shared_gate_weight.shape[1]
    inner_cols = (jax.nn.silu(dense_sum[:, :dense_cols]) * dense_sum[:, dense_cols:]).astype(
        jnp.bfloat16
    )
    dense_inner = lax.all_to_all(inner_cols, "ep", split_axis=0, concat_axis=1, tiled=True)
    dense_out = jnp.dot(dense_inner, shared_down_weight, preferred_element_type=jnp.float32)
    result = hidden_f32 + routed + jax.nn.sigmoid(blend_logit)[:, None] * dense_out
    return (result.astype(jnp.bfloat16), next_re, next_im)


def solution(mesh):
    placed = (
        P("ep", "tp"),
        P("ep", "tp", None),
        P("ep", "tp", None),
        P(),
        P(),
        P("tp", None),
        P("tp", None),
        P("tp"),
        P("tp", None, None),
        P("tp", None, None),
        P("tp", None, None),
        P("tp", None, None),
        P("tp"),
        P("tp", None),
        P("tp", None),
        P(),
        P(),
        P(),
        P("ep", None),
        P("ep", None, "tp"),
        P("ep", None, "tp"),
        P("ep", "tp", None),
        P("tp", "ep"),
        P("tp", "ep"),
        P(None, "tp"),
    )
    return jax.shard_map(
        shards,
        mesh=mesh,
        in_specs=placed,
        out_specs=(P("ep", "tp"), P("ep", "tp", None), P("ep", "tp", None)),
        check_vma=False,
    )
```

profile of v0, /device:TPU:0, one launch (start us, length us, event | category | flops | bytes accessed | tf_op | source)
XLA Modules:
  0.0 187.7 jit_solution(3510667995029894204)
XLA Ops:
  7.2 3.5 %copy.64 = f32[64,64,64]{0,2,1:T(8,128)} copy(f32[64,64,64]{2,1,0:T(8,128)} %param.27) | data formatting | bytes 2097152 | tf_op args[2]
  10.7 3.4 %copy.63 = f32[64,64,64]{0,2,1:T(8,128)} copy(f32[64,64,64]{2,1,0:T(8,128)} %param.26) | data formatting | bytes 2097152 | tf_op args[1]
  14.3 2.6 %psum.35 = f32[64]{0:T(128)S(1)} all-reduce(f32[64]{0:T(128)S(1)} %fusion.29), channel_id=1, replica_groups=mesh['ep'=16,'tp'=2] {'tp'}, use_global_device_ids=true, to_apply=%region_1.0 | all-reduce | flops 64 | bytes 512 | tf_op jit(solution)/shard_map/psum | solution.py:91
  19.8 4.9 %bitcast_add_fusion.1 = f32[64,64,64]{0,2,1:T(8,128)S(1)} fusion(f32[64,64,64]{0,2,1:T(8,128)} %copy.64, f32[64,64,64]{0,2,1:T(8,128)} %copy.63, bf16[64,64,16]{0,2,1:T(8,128)(2,1)S(1)} %bitcast.75, f32[64,64]{1,0:T(8,128)S(1)} %get-tuple-element.17, f32[64,64]{1,0:T(8,128)S(1)} %get-tuple-element.18, f32[64,64,16]{1,2,0:T(8,128)S(1)} %copy-done.7, ...), kind=kOutput, calls=%fused_computation.13 | convolution fusion | flops 51576832 | bytes 3866624 | tf_op jit(solution)/shard_map/tgc,gpc->tgp/dot_general | solution.py:38
  24.8 3.2 %bitcast_add_fusion = f32[64,64,64]{0,2,1:T(8,128)S(1)} fusion(f32[64,64,64]{0,2,1:T(8,128)S(1)} %copy-done.4, f32[64,64,64]{0,2,1:T(8,128)S(1)} %copy-done.3, bf16[64,64,16]{0,2,1:T(8,128)(2,1)S(1)} %bitcast.76, f32[64,64]{1,0:T(8,128)S(1)} %get-tuple-element.17, f32[64,64]{1,0:T(8,128)S(1)} %get-tuple-element.18, f32[64,64,16]{1,2,0:T(8,128)S(1)} %copy-done.8, ...), kind=kOutput, calls=%fused_computation.12 | convolution fusion | flops 51576832 | bytes 3866624 | tf_op jit(solution)/shard_map/tgc,gpc->tgp/dot_general | solution.py:39
  30.0 1.9 %convolution_subtract_fusion = f32[64,64,16]{1,2,0:T(8,128)S(1)} fusion(f32[64,64,16]{1,2,0:T(8,128)S(1)} %fusion.77, f32[64,64,64]{0,2,1:T(8,128)S(1)} %bitcast_add_fusion, f32[64,16,64]{2,1,0:T(8,128)S(1)} %copy-done.10), kind=kOutput, calls=%fused_computation.15 | convolution fusion | flops 50397184 | bytes 1835008 | tf_op jit(solution)/shard_map/dor,zdr->zdo/dot_general | solution.py:43
  32.1 3.3 %fusion.1 = bf16[64,1,2048]{2,0,1:T(8,128)(2,1)S(1)} fusion(bf16[1024,2048]{1,0:T(8,128)(2,1)} %param.39, f32[64,1024]{1,0:T(8,128)S(1)} %copy.70, f32[1024]{0:T(1024)S(1)} %copy-done.14, f32[1024]{0:T(1024)S(1)} %dynamic_slice.15, f32[64]{0:T(128)S(1)} %add_rsqrt_fusion.1, bf16[64,1024]{1,0:T(8,128)(2,1)S(1)} %copy-done.6), kind=kOutput, calls=%fused_computation.6 | convolution fusion | flops 269615104 | bytes 4858112 | tf_op jit(solution)/shard_map/dot_general | solution.py:106
  37.8 10.3 %reduce-scatter.3.cloned.1.call-done = bf16[64,2,1024]{2,0,1:T(8,128)(2,1)} async-done(((bf16[64,2,2048]{2,0,1:T(8,128)(2,1)}), bf16[64,2,1024]{2,0,1:T(8,128)(2,1)}) %reduce-scatter.3.cloned.1.call-update) | async-done | bytes 262160 | tf_op jit(solution)/shard_map/reduce_scatter | solution.py:108
  49.3 2.5 %psum.36 = f32[64]{0:T(128)S(1)} all-reduce(f32[64]{0:T(128)S(1)} %get-tuple-element.14), channel_id=1, replica_groups=mesh['ep'=16,'tp'=2] {'tp'}, use_global_device_ids=true, to_apply=%region_4.0 | all-reduce | flops 64 | bytes 512 | tf_op jit(solution)/shard_map/psum | solution.py:120
  53.4 2.3 %all_gather.6 = bf16[64,2048]{1,0:T(8,128)(2,1)S(1)} all-gather(bf16[64,1024]{1,0:T(8,128)(2,1)} %fusion.43), channel_id=1, replica_groups=mesh['ep'=16,'tp'=2] {'tp'}, dimensions={1}, use_global_device_ids=true | all-gather | bytes 393216 | tf_op jit(solution)/shard_map/all_gather | solution.py:137
  56.2 41.0 %all_to_all.29 = bf16[16,16,2048]{2,1,0:T(8,128)(2,1)S(1)} all-to-all(bf16[16,16,2048]{2,1,0:T(8,128)(2,1)S(1)} %bitcast.74), channel_id=1, replica_groups=mesh['ep'=16,'tp'=2] {'ep'}, dimensions={0} | all-to-all | bytes 2097152 | tf_op jit(solution)/shard_map/all_to_all | solution.py:153
  98.9 4.2 %convolution_convert_fusion = bf16[256,2048]{1,0:T(8,128)(2,1)} fusion(bf16[1,512,2048]{2,1,0:T(8,128)(2,1)S(1)} %copy-done, bf16[256,2048]{1,0:T(8,128)(2,1)} %bitcast.79, bf16[1,2048,512]{2,1,0:T(8,128)(2,1)} %param.45, f32[256,512]{1,0:T(8,128)S(1)} %fusion.5), kind=kOutput, calls=%fused_computation.1 | convolution fusion | flops 1075052544 | bytes 6815744 | tf_op jit(solution)/shard_map/dot_general | solution.py:160
  103.1 3.8 %copy.77 = f32[64,64,64]{2,1,0:T(8,128)} copy(f32[64,64,64]{0,2,1:T(8,128)} %copy-done.2) | data formatting | bytes 2097152
  106.9 3.8 %copy.78 = f32[64,64,64]{2,1,0:T(8,128)} copy(f32[64,64,64]{0,2,1:T(8,128)} %copy-done.1) | data formatting | bytes 2097152
  111.7 3.3 %all-reduce = (f32[64,20]{0,1:T(8,128)S(1)}, f32[64]{0:T(128)S(1)}) all-reduce(f32[64,20]{0,1:T(8,128)S(1)} %fusion.44, f32[64]{0:T(128)S(1)} %convolution_bitcast_fusion), channel_id=1, replica_groups=mesh['ep'=16,'tp'=2] {'tp'}, use_global_device_ids=true, to_apply=%region_5.0 | all-reduce | flops 1344 | bytes 10752 | tf_op jit(solution)/shard_map/psum | solution.py:125
  115.1 3.4 %all-gather.2.cloned.1.call-done = bf16[1024,1024]{1,0:T(8,128)(2,1)} async-done(((bf16[64,1024]{1,0:T(8,128)(2,1)}), bf16[1024,1024]{1,0:T(8,128)(2,1)}) %all-gather.2.cloned.1.call-update) | async-done | bytes 2097168 | tf_op jit(solution)/shard_map/all_gather | solution.py:168
  118.5 2.4 %convolution_convert_fusion.4 = bf16[1024,128]{0,1:T(8,128)(2,1)S(1)} fusion(bf16[1024,1024]{1,0:T(8,128)(2,1)} %all-gather.2.cloned.1.call-done, bf16[1024,128]{1,0:T(8,128)(2,1)S(1)} %copy-done.12), kind=kOutput, calls=%fused_computation.17 | convolution fusion | flops 268566528 | bytes 2621440 | tf_op jit(solution)/shard_map/dot_general | solution.py:52
  120.9 7.1 %reduce-scatter.5.cloned.1.call-done = bf16[256,1024]{1,0:T(8,128)(2,1)} async-done(((bf16[256,2048]{1,0:T(8,128)(2,1)}), bf16[256,1024]{1,0:T(8,128)(2,1)}) %reduce-scatter.5.cloned.1.call-update) | async-done | bytes 524304 | tf_op jit(solution)/shard_map/reduce_scatter | solution.py:161
  128.0 6.8 %all-to-all-start.1 = ((bf16[16,16,1024]{2,1,0:T(8,128)(2,1)}), bf16[16,16,1024]{2,1,0:T(8,128)(2,1)S(1)}, u32[]{:S(2)}, u32[]{:S(2)}) async-start(bf16[16,16,1024]{2,1,0:T(8,128)(2,1)} %bitcast.80), calls=%async_computation.3 | async-start | bytes 1048576 | tf_op jit(solution)/shard_map/all_to_all | solution.py:163
  134.9 2.4 %convolution_convert_fusion.5 = bf16[1024,128]{0,1:T(8,128)(2,1)S(1)} fusion(bf16[1024,1024]{1,0:T(8,128)(2,1)} %all-gather.2.cloned.1.call-done, bf16[1024,128]{1,0:T(8,128)(2,1)S(1)} %copy-done.13), kind=kOutput, calls=%fused_computation.18 | convolution fusion | flops 268566528 | bytes 2621440 | tf_op jit(solution)/shard_map/dot_general | solution.py:51
  138.2 20.0 %all-reduce.3.cloned.1.call-done = bf16[1024,256]{0,1:T(8,128)(2,1)} async-done(((bf16[1024,256]{0,1:T(8,128)(2,1)}), bf16[1024,256]{0,1:T(8,128)(2,1)}) %all-reduce.3.cloned.1.call-update) | async-done | bytes 524304 | tf_op jit(solution)/shard_map/psum | solution.py:170
  160.3 6.8 %all-to-all-start.2 = ((bf16[16,64,128]{2,1,0:T(8,128)(2,1)}), bf16[16,64,128]{2,1,0:T(8,128)(2,1)S(1)}, u32[]{:S(2)}, u32[]{:S(2)}) async-start(bf16[16,64,128]{2,1,0:T(8,128)(2,1)} %bitcast.19), calls=%async_computation.4 | async-start | bytes 524288 | tf_op jit(solution)/shard_map/all_to_all | solution.py:175
  169.2 8.2 %all-to-all-done.2 = bf16[16,64,128]{2,1,0:T(8,128)(2,1)S(1)} async-done(((bf16[16,64,128]{2,1,0:T(8,128)(2,1)}), bf16[16,64,128]{2,1,0:T(8,128)(2,1)S(1)}, u32[]{:S(2)}, u32[]{:S(2)}) %all-to-all-start.2) | async-done | bytes 262176 | tf_op jit(solution)/shard_map/all_to_all | solution.py:175
  177.5 3.7 %fusion.14 = bf16[64,1024]{1,0:T(8,128)(2,1)} fusion(bf16[2048,1024]{1,0:T(8,128)(2,1)} %param.49, f32[64,1024]{1,0:T(8,128)S(1)} %multiply_reduce_fusion, bf16[64,1024]{1,0:T(8,128)(2,1)S(1)} %get-tuple-element.15, f32[64]{0:T(128)S(1)} %add_divide_fusion, bf16[16,64,128]{2,1,0:T(8,128)(2,1)S(1)} %all-to-all-done.2), kind=kOutput, calls=%fused_computation.21 | convolution fusion | flops 268763136 | bytes 4980992 | tf_op jit(solution)/shard_map/dot_general | solution.py:176
  (109 shorter events, 18.4 us)
Async XLA Ops:
  7.2 91.7 %copy-start = (bf16[1,512,2048]{2,1,0:T(8,128)(2,1)S(1)}, bf16[1,512,2048]{2,1,0:T(8,128)(2,1)}, u32[]{:S(2)}) copy-start(bf16[1,512,2048]{2,1,0:T(8,128)(2,1)} %param.46) | copy-start | bytes 6291460
  7.2 40.9 %reduce-scatter.3.cloned.1.call-start = ((), (), s32[]{:S(2)}) async-start(), calls=%async_computation.5 | async-start | bytes 786432 | tf_op jit(solution)/shard_map/reduce_scatter | solution.py:108
  10.7 3.4 %copy-start.6 = (bf16[64,1024]{1,0:T(8,128)(2,1)S(1)}, bf16[64,1024]{1,0:T(8,128)(2,1)}, u32[]{:S(2)}) copy-start(bf16[64,1024]{1,0:T(8,128)(2,1)} %param.25) | copy-start | bytes 393220
  10.7 6.2 %copy-start.18 = (f32[2048]{0:T(1024)S(1)}, f32[2048]{0:T(1024)}, u32[]{:S(2)}) copy-start(f32[2048]{0:T(1024)} %param.28) | copy-start | bytes 24580
  10.7 8.0 %copy-start.21 = (f32[64]{0:T(128)S(1)}, f32[64]{0:T(128)}, u32[]{:S(2)}) copy-start(f32[64]{0:T(128)} %param.32) | copy-start | bytes 772
  10.7 9.1 %copy-start.7 = (f32[64,64,16]{1,2,0:T(8,128)S(1)}, f32[64,64,16]{1,2,0:T(8,128)}, u32[]{:S(2)}) copy-start(f32[64,64,16]{1,2,0:T(8,128)} %param.34) | copy-start | bytes 786436
  10.7 9.1 %copy-start.8 = (f32[64,64,16]{1,2,0:T(8,128)S(1)}, f32[64,64,16]{1,2,0:T(8,128)}, u32[]{:S(2)}) copy-start(f32[64,64,16]{1,2,0:T(8,128)} %param.33) | copy-start | bytes 786436
  19.8 5.0 %copy-start.3 = (f32[64,64,64]{0,2,1:T(8,128)S(1)}, f32[64,64,64]{0,2,1:T(8,128)}, u32[]{:S(2)}) copy-start(f32[64,64,64]{0,2,1:T(8,128)} %copy.64) | copy-start | bytes 3145732
  19.8 5.0 %copy-start.4 = (f32[64,64,64]{0,2,1:T(8,128)S(1)}, f32[64,64,64]{0,2,1:T(8,128)}, u32[]{:S(2)}) copy-start(f32[64,64,64]{0,2,1:T(8,128)} %copy.63) | copy-start | bytes 3145732
  24.8 3.3 %copy-start.2 = (f32[64,64,64]{0,2,1:T(8,128)}, f32[64,64,64]{0,2,1:T(8,128)S(1)}, u32[]{:S(2)}) copy-start(f32[64,64,64]{0,2,1:T(8,128)S(1)} %bitcast_add_fusion.1) | copy-start | bytes 3145732
  24.8 3.3 %copy-start.11 = (f32[64,16,64]{2,1,0:T(8,128)S(1)}, f32[64,16,64]{2,1,0:T(8,128)}, u32[]{:S(2)}) copy-start(f32[64,16,64]{2,1,0:T(8,128)} %param.35) | copy-start | bytes 786436
  28.0 3.9 %copy-start.1 = (f32[64,64,64]{0,2,1:T(8,128)}, f32[64,64,64]{0,2,1:T(8,128)S(1)}, u32[]{:S(2)}) copy-start(f32[64,64,64]{0,2,1:T(8,128)S(1)} %bitcast_add_fusion) | copy-start | bytes 3145732
  32.1 3.5 %copy-start.5 = (bf16[1024,2048]{1,0:T(8,128)(2,1)S(1)}, bf16[1024,2048]{1,0:T(8,128)(2,1)}, u32[]{:S(2)}) copy-start(bf16[1024,2048]{1,0:T(8,128)(2,1)} %param.38) | copy-start | bytes 12582916
  37.4 81.1 %all-gather.2.cloned.1.call-start = ((), (), s32[]{:S(2)}) async-start(), calls=%async_computation.7 | async-start | bytes 2228224 | tf_op jit(solution)/shard_map/all_gather | solution.py:168
  52.5 75.5 %reduce-scatter.5.cloned.1.call-start = ((), (), s32[]{:S(2)}) async-start(), calls=%async_computation.6 | async-start | bytes 1572864 | tf_op jit(solution)/shard_map/reduce_scatter | solution.py:161
  53.3 44.9 %copy-start.20 = (bf16[1,2048,512]{2,1,0:T(8,128)(2,1)S(1)}, bf16[1,2048,512]{2,1,0:T(8,128)(2,1)}, u32[]{:S(2)}) copy-start(bf16[1,2048,512]{2,1,0:T(8,128)(2,1)} %param.44) | copy-start | bytes 6291460
  106.9 4.0 %copy-start.17 = (bf16[2048,4]{0,1:T(4,128)(2,1)S(1)}, bf16[2048,4]{0,1:T(4,128)(2,1)}, u32[]{:S(2)}) copy-start(bf16[2048,4]{0,1:T(4,128)(2,1)} %param.40) | copy-start | bytes 49156
  106.9 4.0 %copy-start.15 = (bf16[2048,16]{0,1:T(8,128)(2,1)S(1)}, bf16[2048,16]{0,1:T(8,128)(2,1)}, u32[]{:S(2)}) copy-start(bf16[2048,16]{0,1:T(8,128)(2,1)} %param.41) | copy-start | bytes 196612
  106.9 4.1 %dynamic-slice-start = ((f32[2048]{0:T(1024)}, s32[]{:T(128)}), f32[1024]{0:T(1024)S(1)}, s32[]{:S(2)}) async-start(f32[2048]{0:T(1024)} %param.42, s32[]{:T(128)} %select_n.30), calls=%async_computation.9 | async-start | bytes 8704 | tf_op jit(solution)/shard_map/dynamic_slice | solution.py:88
  106.9 11.6 %copy-start.12 = (bf16[1024,128]{1,0:T(8,128)(2,1)S(1)}, bf16[1024,128]{1,0:T(8,128)(2,1)}, u32[]{:S(2)}) copy-start(bf16[1024,128]{1,0:T(8,128)(2,1)} %param.48) | copy-start | bytes 786436
  111.0 23.9 %copy-start.13 = (bf16[1024,128]{1,0:T(8,128)(2,1)S(1)}, bf16[1024,128]{1,0:T(8,128)(2,1)}, u32[]{:S(2)}) copy-start(bf16[1024,128]{1,0:T(8,128)(2,1)} %param.47) | copy-start | bytes 786436
  128.0 32.3 %all-to-all-start.1 = ((bf16[16,16,1024]{2,1,0:T(8,128)(2,1)}), bf16[16,16,1024]{2,1,0:T(8,128)(2,1)S(1)}, u32[]{:S(2)}, u32[]{:S(2)}) async-start(bf16[16,16,1024]{2,1,0:T(8,128)(2,1)} %bitcast.80), calls=%async_computation.3 | async-start | bytes 1048576 | tf_op jit(solution)/shard_map/all_to_all | solution.py:163
  134.8 23.4 %all-reduce.3.cloned.1.call-start = ((), (), s32[]{:S(2)}) async-start(), calls=%async_computation.8 | async-start | bytes 1048576 | tf_op jit(solution)/shard_map/psum | solution.py:170
  160.3 17.1 %all-to-all-start.2 = ((bf16[16,64,128]{2,1,0:T(8,128)(2,1)}), bf16[16,64,128]{2,1,0:T(8,128)(2,1)S(1)}, u32[]{:S(2)}, u32[]{:S(2)}) async-start(bf16[16,64,128]{2,1,0:T(8,128)(2,1)} %bitcast.19), calls=%async_computation.4 | async-start | bytes 524288 | tf_op jit(solution)/shard_map/all_to_all | solution.py:175
  (5 other events, 8.9 us)
Sparse Core Ops, SparseCore 0:
  37.6 10.4 reduce-scatter.2
  52.6 65.8 all-gather.1
  120.8 7.2 reduce-scatter.4
  138.3 19.8 all-reduce.2
where the time goes:
time: 188 us
  blocking collectives  51.7 us (28%)
  waiting for transfers between devices  49.1 us (26%)
  matrix products  30.9 us (16%)
  local copies, waits for them, and re-layouts  19.7 us (10%)
  between operations  14.3 us (8%)
  starting transfers between devices  13.8 us (7%)
  other arithmetic  8.23 us (4%)
    all_to_all x1, blocking collectives, shards(): lax.all_to_all(outgoing, 'ep', split_axis=0, concat_axis=0, tiled=True)  41 us
    psum x1, waiting for transfers between devices, shards(): lax.psum(partial_dense.astype(jnp.bfloat16), 'tp').astype(jnp.float32)  20 us
    unnamed x49, local copies, waits for them, and re-layouts  15.8 us
    reduce_scatter x1, waiting for transfers between devices, shards(): lax.psum_scatter(stacked.astype(jnp.bfloat16), 'tp', scatter_dimension=2,...  10.3 us
    all_to_all x1, waiting for transfers between devices, shards(): lax.all_to_all(inner_cols, 'ep', split_axis=0, concat_axis=1, tiled=True)  8.24 us
    reduce_scatter x1, waiting for transfers between devices, shards(): lax.psum_scatter(part_out.astype(jnp.bfloat16), 'tp', scatter_dimension=1...  7.08 us
    all_to_all x1, starting transfers between devices, shards(): lax.all_to_all(inner_cols, 'ep', split_axis=0, concat_axis=1, tiled=True)  6.83 us
    all_to_all x1, starting transfers between devices, shards(): lax.all_to_all(finished, 'ep', split_axis=0, concat_axis=0, tiled=True)  6.79 us
  transfers between devices with their start and end apart: 6, of which 5 were waited for; matrix products, arithmetic and copies ran while one was open for 13% of the time, Pallas kernels for 0%

commit v1 on v0

--- a/solution.py
+++ b/solution.py
@@ -172,7 +172,9 @@
     inner_cols = (jax.nn.silu(dense_sum[:, :dense_cols]) * dense_sum[:, dense_cols:]).astype(
         jnp.bfloat16
     )
-    dense_inner = lax.all_to_all(inner_cols, "ep", split_axis=0, concat_axis=1, tiled=True)
+    pieces = jnp.split(inner_cols, lax.axis_size("ep"), axis=0)
+    arrived = lax.all_to_all(jnp.stack(pieces), "ep", 0, 0)
+    dense_inner = jnp.concatenate(arrived, axis=1)
     dense_out = jnp.dot(dense_inner, shared_down_weight, preferred_element_type=jnp.float32)
     result = hidden_f32 + routed + jax.nn.sigmoid(blend_logit)[:, None] * dense_out
     return (result.astype(jnp.bfloat16), next_re, next_im)

time: 188 us -> 180 us (0.957)
  waiting for transfers between devices: 49.1 us -> 41 us
    psum x1, waiting for transfers between devices: 20 us -> 15.2 us  [shards(): lax.psum(partial_dense.astype(jnp.bfloat16), 'tp').astype(jnp.float32)]
    reduce_scatter x1, waiting for transfers between devices: 7.08 us -> 5.09 us  [shards(): lax.psum_scatter(part_out.astype(jnp.bfloat16), 'tp', scatter_dimension=1...]
    unnamed x49 -> x66, local copies, waits for them, and re-layouts: 15.8 us -> 16.6 us
  transfers between devices with their start and end apart: 6 -> 6, of which waited for: 5 -> 5; matrix products, arithmetic and copies ran while one was open for 13% -> 14% of each run, Pallas kernels for 0% -> 0%
where the time goes in v1:
time: 180 us
  blocking collectives  51.9 us (29%)
  waiting for transfers between devices  41 us (23%)
  matrix products  29.7 us (16%)
  local copies, waits for them, and re-layouts  20.7 us (12%)
  between operations  14.4 us (8%)
  starting transfers between devices  13.8 us (8%)
  other arithmetic  8.23 us (5%)
    all_to_all x1, blocking collectives, shards(): lax.all_to_all(outgoing, 'ep', split_axis=0, concat_axis=0, tiled=True)  41.1 us
    unnamed x66, local copies, waits for them, and re-layouts  16.6 us
    psum x1, waiting for transfers between devices, shards(): lax.psum(partial_dense.astype(jnp.bfloat16), 'tp').astype(jnp.float32)  15.2 us
    reduce_scatter x1, waiting for transfers between devices, shards(): lax.psum_scatter(stacked.astype(jnp.bfloat16), 'tp', scatter_dimension=2,...  10.3 us
    all_to_all x1, waiting for transfers between devices, shards(): arrived = lax.all_to_all(jnp.stack(pieces), 'ep', 0, 0)  8.24 us
    all_to_all x1, starting transfers between devices, shards(): arrived = lax.all_to_all(jnp.stack(pieces), 'ep', 0, 0)  6.83 us
    all_to_all x1, starting transfers between devices, shards(): lax.all_to_all(finished, 'ep', split_axis=0, concat_axis=0, tiled=True)  6.79 us
    reduce_scatter x1, waiting for transfers between devices, shards(): lax.psum_scatter(part_out.astype(jnp.bfloat16), 'tp', scatter_dimension=1...  5.09 us
  transfers between devices with their start and end apart: 6, of which 5 were waited for; matrix products, arithmetic and copies ran while one was open for 14% of the time, Pallas kernels for 0%

profile of v1, /device:TPU:0, one launch (start us, length us, event | category | flops | bytes accessed | tf_op | source)
XLA Modules:
  0.0 179.6 jit_solution(15755570435059114700)
XLA Ops:
  7.2 3.5 %copy.97 = f32[64,64,64]{0,2,1:T(8,128)} copy(f32[64,64,64]{2,1,0:T(8,128)} %param.27) | data formatting | bytes 2097152 | tf_op args[2]
  10.7 3.4 %copy.96 = f32[64,64,64]{0,2,1:T(8,128)} copy(f32[64,64,64]{2,1,0:T(8,128)} %param.26) | data formatting | bytes 2097152 | tf_op args[1]
  14.3 2.6 %psum.35 = f32[64]{0:T(128)S(1)} all-reduce(f32[64]{0:T(128)S(1)} %fusion.29), channel_id=1, replica_groups=mesh['ep'=16,'tp'=2] {'tp'}, use_global_device_ids=true, to_apply=%region_1.0 | all-reduce | flops 64 | bytes 512 | tf_op jit(solution)/shard_map/psum | solution.py:91
  19.8 4.9 %bitcast_add_fusion.1 = f32[64,64,64]{0,2,1:T(8,128)S(1)} fusion(f32[64,64,64]{0,2,1:T(8,128)} %copy.97, f32[64,64,64]{0,2,1:T(8,128)} %copy.96, bf16[64,64,16]{0,2,1:T(8,128)(2,1)S(1)} %bitcast.138, f32[64,64]{1,0:T(8,128)S(1)} %get-tuple-element.23, f32[64,64]{1,0:T(8,128)S(1)} %get-tuple-element.24, f32[64,64,16]{1,2,0:T(8,128)S(1)} %copy-done.8, ...), kind=kOutput, calls=%fused_computation.13 | convolution fusion | flops 51576832 | bytes 3866624 | tf_op jit(solution)/shard_map/tgc,gpc->tgp/dot_general | solution.py:38
  24.8 3.2 %bitcast_add_fusion = f32[64,64,64]{0,2,1:T(8,128)S(1)} fusion(f32[64,64,64]{0,2,1:T(8,128)S(1)} %copy-done.4, f32[64,64,64]{0,2,1:T(8,128)S(1)} %copy-done.3, bf16[64,64,16]{0,2,1:T(8,128)(2,1)S(1)} %bitcast.139, f32[64,64]{1,0:T(8,128)S(1)} %get-tuple-element.23, f32[64,64]{1,0:T(8,128)S(1)} %get-tuple-element.24, f32[64,64,16]{1,2,0:T(8,128)S(1)} %copy-done.9, ...), kind=kOutput, calls=%fused_computation.12 | convolution fusion | flops 51576832 | bytes 3866624 | tf_op jit(solution)/shard_map/tgc,gpc->tgp/dot_general | solution.py:39
  28.1 1.9 %fusion.93 = f32[64,64,16]{1,2,0:T(8,128)S(1)} fusion(f32[64,64,64]{0,2,1:T(8,128)S(1)} %bitcast_add_fusion.1, f32[64,16,64]{2,1,0:T(8,128)S(1)} %copy-done.12), kind=kOutput, calls=%fused_computation.155 | convolution fusion | flops 50331648 | bytes 1572864 | tf_op jit(solution)/shard_map/dor,zdr->zdo/dot_general | solution.py:42
  30.0 1.9 %convolution_subtract_fusion = f32[64,64,16]{1,2,0:T(8,128)S(1)} fusion(f32[64,64,16]{1,2,0:T(8,128)S(1)} %fusion.93, f32[64,64,64]{0,2,1:T(8,128)S(1)} %bitcast_add_fusion, f32[64,16,64]{2,1,0:T(8,128)S(1)} %copy-done.11), kind=kOutput, calls=%fused_computation.15 | convolution fusion | flops 50397184 | bytes 1835008 | tf_op jit(solution)/shard_map/dor,zdr->zdo/dot_general | solution.py:43
  32.1 3.3 %fusion.1 = bf16[64,1,2048]{2,0,1:T(8,128)(2,1)S(1)} fusion(bf16[1024,2048]{1,0:T(8,128)(2,1)} %param.39, f32[64,1024]{1,0:T(8,128)S(1)} %copy.103, f32[1024]{0:T(1024)S(1)} %copy-done.15, f32[1024]{0:T(1024)S(1)} %dynamic_slice.15, f32[64]{0:T(128)S(1)} %add_rsqrt_fusion.1, bf16[64,1024]{1,0:T(8,128)(2,1)S(1)} %copy-done.7), kind=kOutput, calls=%fused_computation.6 | convolution fusion | flops 269615104 | bytes 4858112 | tf_op jit(solution)/shard_map/dot_general | solution.py:106
  37.8 10.3 %reduce-scatter.3.cloned.1.call-done = bf16[64,2,1024]{2,0,1:T(8,128)(2,1)} async-done(((bf16[64,2,2048]{2,0,1:T(8,128)(2,1)}), bf16[64,2,1024]{2,0,1:T(8,128)(2,1)}) %reduce-scatter.3.cloned.1.call-update) | async-done | bytes 262160 | tf_op jit(solution)/shard_map/reduce_scatter | solution.py:108
  49.3 2.5 %psum.36 = f32[64]{0:T(128)S(1)} all-reduce(f32[64]{0:T(128)S(1)} %get-tuple-element.20), channel_id=1, replica_groups=mesh['ep'=16,'tp'=2] {'tp'}, use_global_device_ids=true, to_apply=%region_4.0 | all-reduce | flops 64 | bytes 512 | tf_op jit(solution)/shard_map/psum | solution.py:120
  53.4 2.3 %all_gather.6 = bf16[64,2048]{1,0:T(8,128)(2,1)S(1)} all-gather(bf16[64,1024]{1,0:T(8,128)(2,1)} %fusion.43), channel_id=1, replica_groups=mesh['ep'=16,'tp'=2] {'tp'}, dimensions={1}, use_global_device_ids=true | all-gather | bytes 393216 | tf_op jit(solution)/shard_map/all_gather | solution.py:137
  56.2 41.1 %all_to_all.15 = bf16[16,16,2048]{2,1,0:T(8,128)(2,1)S(1)} all-to-all(bf16[16,16,2048]{2,1,0:T(8,128)(2,1)S(1)} %bitcast.137), channel_id=1, replica_groups=mesh['ep'=16,'tp'=2] {'ep'}, dimensions={0} | all-to-all | bytes 2097152 | tf_op jit(solution)/shard_map/all_to_all | solution.py:153
  99.0 4.5 %convolution_convert_fusion = bf16[256,2048]{1,0:T(8,128)(2,1)} fusion(bf16[1,512,2048]{2,1,0:T(8,128)(2,1)S(1)} %copy-done, bf16[256,2048]{1,0:T(8,128)(2,1)} %bitcast.142, bf16[1,2048,512]{2,1,0:T(8,128)(2,1)} %param.45, f32[256,512]{1,0:T(8,128)S(1)} %fusion.5), kind=kOutput, calls=%fused_computation.1 | convolution fusion | flops 1075052544 | bytes 6815744 | tf_op jit(solution)/shard_map/dot_general | solution.py:160
  103.6 3.8 %copy.110 = f32[64,64,64]{2,1,0:T(8,128)} copy(f32[64,64,64]{0,2,1:T(8,128)} %copy-done.2) | data formatting | bytes 2097152
  107.4 3.8 %copy.111 = f32[64,64,64]{2,1,0:T(8,128)} copy(f32[64,64,64]{0,2,1:T(8,128)} %copy-done.1) | data formatting | bytes 2097152
  112.2 3.3 %all-reduce = (f32[64,20]{0,1:T(8,128)S(1)}, f32[64]{0:T(128)S(1)}) all-reduce(f32[64,20]{0,1:T(8,128)S(1)} %fusion.44, f32[64]{0:T(128)S(1)} %convolution_bitcast_fusion), channel_id=1, replica_groups=mesh['ep'=16,'tp'=2] {'tp'}, use_global_device_ids=true, to_apply=%region_5.0 | all-reduce | flops 1344 | bytes 10752 | tf_op jit(solution)/shard_map/psum | solution.py:125
  115.5 2.1 %all-gather.2.cloned.1.call-done = bf16[1024,1024]{1,0:T(8,128)(2,1)} async-done(((bf16[64,1024]{1,0:T(8,128)(2,1)}), bf16[1024,1024]{1,0:T(8,128)(2,1)}) %all-gather.2.cloned.1.call-update) | async-done | bytes 2097168 | tf_op jit(solution)/shard_map/all_gather | solution.py:168
  117.6 2.6 %convolution_convert_fusion.4 = bf16[1024,128]{0,1:T(8,128)(2,1)S(1)} fusion(bf16[1024,1024]{1,0:T(8,128)(2,1)} %all-gather.2.cloned.1.call-done, bf16[1024,128]{1,0:T(8,128)(2,1)S(1)} %copy-done.13), kind=kOutput, calls=%fused_computation.17 | convolution fusion | flops 268566528 | bytes 2621440 | tf_op jit(solution)/shard_map/dot_general | solution.py:52
  122.0 5.1 %reduce-scatter.5.cloned.1.call-done = bf16[256,1024]{1,0:T(8,128)(2,1)} async-done(((bf16[256,2048]{1,0:T(8,128)(2,1)}), bf16[256,1024]{1,0:T(8,128)(2,1)}) %reduce-scatter.5.cloned.1.call-update) | async-done | bytes 524304 | tf_op jit(solution)/shard_map/reduce_scatter | solution.py:161
  127.1 6.8 %all-to-all-start.1 = ((bf16[16,16,1024]{2,1,0:T(8,128)(2,1)}), bf16[16,16,1024]{2,1,0:T(8,128)(2,1)S(1)}, u32[]{:S(2)}, u32[]{:S(2)}) async-start(bf16[16,16,1024]{2,1,0:T(8,128)(2,1)} %bitcast.143), calls=%async_computation.3 | async-start | bytes 1048576 | tf_op jit(solution)/shard_map/all_to_all | solution.py:163
  133.9 15.2 %all-reduce.3.cloned.1.call-done = bf16[1024,256]{0,1:T(8,128)(2,1)} async-done(((bf16[1024,256]{0,1:T(8,128)(2,1)}), bf16[1024,256]{0,1:T(8,128)(2,1)}) %all-reduce.3.cloned.1.call-update) | async-done | bytes 524304 | tf_op jit(solution)/shard_map/psum | solution.py:170
  152.3 6.8 %all-to-all-start.2 = ((bf16[16,64,128]{2,1,0:T(8,128)(2,1)}), bf16[16,64,128]{2,1,0:T(8,128)(2,1)S(1)}, u32[]{:S(2)}, u32[]{:S(2)}) async-start(bf16[16,64,128]{2,1,0:T(8,128)(2,1)} %copy.108), calls=%async_computation.4 | async-start | bytes 524288 | tf_op jit(solution)/shard_map/all_to_all | solution.py:176
  161.2 8.2 %all-to-all-done.2 = bf16[16,64,128]{2,1,0:T(8,128)(2,1)S(1)} async-done(((bf16[16,64,128]{2,1,0:T(8,128)(2,1)}), bf16[16,64,128]{2,1,0:T(8,128)(2,1)S(1)}, u32[]{:S(2)}, u32[]{:S(2)}) %all-to-all-start.2) | async-done | bytes 262176 | tf_op jit(solution)/shard_map/all_to_all | solution.py:176
  169.4 3.7 %fusion.14 = bf16[64,1024]{1,0:T(8,128)(2,1)} fusion(bf16[2048,1024]{1,0:T(8,128)(2,1)} %param.49, f32[64,1024]{1,0:T(8,128)S(1)} %multiply_reduce_fusion, bf16[64,1024]{1,0:T(8,128)(2,1)S(1)} %get-tuple-element.21, f32[64]{0:T(128)S(1)} %add_divide_fusion, bf16[16,64,128]{2,1,0:T(8,128)(2,1)S(1)} %all-to-all-done.2), kind=kOutput, calls=%fused_computation.21 | convolution fusion | flops 268763136 | bytes 4980992 | tf_op jit(solution)/shard_map/dot_general | solution.py:178
  (127 shorter events, 18.3 us)
Async XLA Ops:
  7.2 91.8 %copy-start = (bf16[1,512,2048]{2,1,0:T(8,128)(2,1)S(1)}, bf16[1,512,2048]{2,1,0:T(8,128)(2,1)}, u32[]{:S(2)}) copy-start(bf16[1,512,2048]{2,1,0:T(8,128)(2,1)} %param.46) | copy-start | bytes 6291460
  7.2 40.9 %reduce-scatter.3.cloned.1.call-start = ((), (), s32[]{:S(2)}) async-start(), calls=%async_computation.5 | async-start | bytes 786432 | tf_op jit(solution)/shard_map/reduce_scatter | solution.py:108
  10.7 3.4 %copy-start.7 = (bf16[64,1024]{1,0:T(8,128)(2,1)S(1)}, bf16[64,1024]{1,0:T(8,128)(2,1)}, u32[]{:S(2)}) copy-start(bf16[64,1024]{1,0:T(8,128)(2,1)} %param.25) | copy-start | bytes 393220
  10.7 6.2 %copy-start.19 = (f32[2048]{0:T(1024)S(1)}, f32[2048]{0:T(1024)}, u32[]{:S(2)}) copy-start(f32[2048]{0:T(1024)} %param.28) | copy-start | bytes 24580
  10.7 8.0 %copy-start.22 = (f32[64]{0:T(128)S(1)}, f32[64]{0:T(128)}, u32[]{:S(2)}) copy-start(f32[64]{0:T(128)} %param.32) | copy-start | bytes 772
  10.7 9.1 %copy-start.8 = (f32[64,64,16]{1,2,0:T(8,128)S(1)}, f32[64,64,16]{1,2,0:T(8,128)}, u32[]{:S(2)}) copy-start(f32[64,64,16]{1,2,0:T(8,128)} %param.34) | copy-start | bytes 786436
  10.7 9.1 %copy-start.9 = (f32[64,64,16]{1,2,0:T(8,128)S(1)}, f32[64,64,16]{1,2,0:T(8,128)}, u32[]{:S(2)}) copy-start(f32[64,64,16]{1,2,0:T(8,128)} %param.33) | copy-start | bytes 786436
  19.8 5.0 %copy-start.3 = (f32[64,64,64]{0,2,1:T(8,128)S(1)}, f32[64,64,64]{0,2,1:T(8,128)}, u32[]{:S(2)}) copy-start(f32[64,64,64]{0,2,1:T(8,128)} %copy.97) | copy-start | bytes 3145732
  19.8 5.0 %copy-start.4 = (f32[64,64,64]{0,2,1:T(8,128)S(1)}, f32[64,64,64]{0,2,1:T(8,128)}, u32[]{:S(2)}) copy-start(f32[64,64,64]{0,2,1:T(8,128)} %copy.96) | copy-start | bytes 3145732
  24.8 3.3 %copy-start.2 = (f32[64,64,64]{0,2,1:T(8,128)}, f32[64,64,64]{0,2,1:T(8,128)S(1)}, u32[]{:S(2)}) copy-start(f32[64,64,64]{0,2,1:T(8,128)S(1)} %bitcast_add_fusion.1) | copy-start | bytes 3145732
  24.8 3.3 %copy-start.12 = (f32[64,16,64]{2,1,0:T(8,128)S(1)}, f32[64,16,64]{2,1,0:T(8,128)}, u32[]{:S(2)}) copy-start(f32[64,16,64]{2,1,0:T(8,128)} %param.35) | copy-start | bytes 786436
  28.0 3.9 %copy-start.1 = (f32[64,64,64]{0,2,1:T(8,128)}, f32[64,64,64]{0,2,1:T(8,128)S(1)}, u32[]{:S(2)}) copy-start(f32[64,64,64]{0,2,1:T(8,128)S(1)} %bitcast_add_fusion) | copy-start | bytes 3145732
  32.1 3.5 %copy-start.6 = (bf16[1024,2048]{1,0:T(8,128)(2,1)S(1)}, bf16[1024,2048]{1,0:T(8,128)(2,1)}, u32[]{:S(2)}) copy-start(bf16[1024,2048]{1,0:T(8,128)(2,1)} %param.38) | copy-start | bytes 12582916
  37.4 80.2 %all-gather.2.cloned.1.call-start = ((), (), s32[]{:S(2)}) async-start(), calls=%async_computation.7 | async-start | bytes 2228224 | tf_op jit(solution)/shard_map/all_gather | solution.py:168
  52.5 74.6 %reduce-scatter.5.cloned.1.call-start = ((), (), s32[]{:S(2)}) async-start(), calls=%async_computation.6 | async-start | bytes 1572864 | tf_op jit(solution)/shard_map/reduce_scatter | solution.py:161
  53.3 45.0 %copy-start.21 = (bf16[1,2048,512]{2,1,0:T(8,128)(2,1)S(1)}, bf16[1,2048,512]{2,1,0:T(8,128)(2,1)}, u32[]{:S(2)}) copy-start(bf16[1,2048,512]{2,1,0:T(8,128)(2,1)} %param.44) | copy-start | bytes 6291460
  103.5 45.6 %all-reduce.3.cloned.1.call-start = ((), (), s32[]{:S(2)}) async-start(), calls=%async_computation.8 | async-start | bytes 1048576 | tf_op jit(solution)/shard_map/psum | solution.py:170
  107.4 4.0 %copy-start.18 = (bf16[2048,4]{0,1:T(4,128)(2,1)S(1)}, bf16[2048,4]{0,1:T(4,128)(2,1)}, u32[]{:S(2)}) copy-start(bf16[2048,4]{0,1:T(4,128)(2,1)} %param.40) | copy-start | bytes 49156
  107.4 4.0 %copy-start.16 = (bf16[2048,16]{0,1:T(8,128)(2,1)S(1)}, bf16[2048,16]{0,1:T(8,128)(2,1)}, u32[]{:S(2)}) copy-start(bf16[2048,16]{0,1:T(8,128)(2,1)} %param.41) | copy-start | bytes 196612
  107.4 4.1 %dynamic-slice-start = ((f32[2048]{0:T(1024)}, s32[]{:T(128)}), f32[1024]{0:T(1024)S(1)}, s32[]{:S(2)}) async-start(f32[2048]{0:T(1024)} %param.42, s32[]{:T(128)} %select_n.30), calls=%async_computation.9 | async-start | bytes 8704 | tf_op jit(solution)/shard_map/dynamic_slice | solution.py:88
  107.4 10.3 %copy-start.13 = (bf16[1024,128]{1,0:T(8,128)(2,1)S(1)}, bf16[1024,128]{1,0:T(8,128)(2,1)}, u32[]{:S(2)}) copy-start(bf16[1024,128]{1,0:T(8,128)(2,1)} %param.48) | copy-start | bytes 786436
  111.2 9.0 %copy-start.14 = (bf16[1024,128]{1,0:T(8,128)(2,1)S(1)}, bf16[1024,128]{1,0:T(8,128)(2,1)}, u32[]{:S(2)}) copy-start(bf16[1024,128]{1,0:T(8,128)(2,1)} %param.47) | copy-start | bytes 786436
  127.1 25.2 %all-to-all-start.1 = ((bf16[16,16,1024]{2,1,0:T(8,128)(2,1)}), bf16[16,16,1024]{2,1,0:T(8,128)(2,1)S(1)}, u32[]{:S(2)}, u32[]{:S(2)}) async-start(bf16[16,16,1024]{2,1,0:T(8,128)(2,1)} %bitcast.143), calls=%async_computation.3 | async-start | bytes 1048576 | tf_op jit(solution)/shard_map/all_to_all | solution.py:163
  152.3 17.1 %all-to-all-start.2 = ((bf16[16,64,128]{2,1,0:T(8,128)(2,1)}), bf16[16,64,128]{2,1,0:T(8,128)(2,1)S(1)}, u32[]{:S(2)}, u32[]{:S(2)}) async-start(bf16[16,64,128]{2,1,0:T(8,128)(2,1)} %copy.108), calls=%async_computation.4 | async-start | bytes 524288 | tf_op jit(solution)/shard_map/all_to_all | solution.py:176
  (6 other events, 11.5 us)
Sparse Core Ops, SparseCore 0:
  37.6 10.4 reduce-scatter.2
  52.6 64.9 all-gather.1
  119.9 7.1 reduce-scatter.4
  129.3 19.7 all-reduce.2
